TPU v7x, 32 devices: a whole 2x2x4 slice. The times are simulated.
32 devices in a mesh: rep: 2 (over x), fs: 8 (over z, y), tp: 2 (over core).
Axes of the slice: x: 2, y: 2, z: 4, core: 2. Of those that a mesh axis runs over, the one named last changes fastest.
Arguments:
- inputs: bfloat16 [8192, 2048], P(('rep', 'fs')), may hold values from -6 to 6
- gain: float32 [2048], replicated, may hold values from 0.1 to 1.9
- gate_weight: bfloat16 [2048, 3072], P('fs', 'tp'), may hold values from -0.125 to 0.125
- up_weight: bfloat16 [2048, 3072], P('fs', 'tp'), may hold values from -0.125 to 0.125
- down_weight: bfloat16 [2048, 3072], P('fs', 'tp'), may hold values from -0.109375 to 0.109375
- cotangent: bfloat16 [8192, 2048], P(('rep', 'fs')), may hold values from -6 to 6
Outputs:
- input_gradient: bfloat16 [8192, 2048], P(('rep', 'fs'))
- gain_gradient: float32 [2048], replicated
- d_down: float32 [2048, 3072], P('fs', 'tp')
All inputs are finite; a program needn't handle non-finite values.
Results may differ from a plain program's by a relative error of at most 0.014.
Values may be sent and summed in bfloat16 or wider, within the bound.
A program may use at most 128 MiB of HBM per device.

v0:
```python
import jax
import jax.numpy as jnp
from jax import lax
from jax.sharding import PartitionSpec as P

EPS = 1e-06


def local(inputs, gain, gate_weight, up_weight, down_weight, cotangent):
    single_precision = inputs.astype(jnp.float32)
    reciprocal_root_mean = lax.rsqrt(
        jnp.mean(single_precision * single_precision, axis=-1, keepdims=True) + EPS
    )
    unit_input = single_precision * reciprocal_root_mean
    normalized_input = (unit_input * gain).astype(jnp.bfloat16)
    row_count = inputs.shape[0]
    contract_cols = (((1,), (1,)), ((), ()))
    gate_full, up_full, down_full = (
        lax.all_gather(gate_weight, "fs", axis=0, tiled=True),
        lax.all_gather(up_weight, "fs", axis=0, tiled=True),
        lax.all_gather(down_weight, "fs", axis=0, tiled=True),
    )
    gate = jnp.dot(normalized_input, gate_full, preferred_element_type=jnp.float32)
    up_proj = jnp.dot(normalized_input, up_full, preferred_element_type=jnp.float32)
    down_sum = jnp.dot(cotangent, down_full, preferred_element_type=jnp.float32)
    gate_sig = jax.nn.sigmoid(gate)
    active = gate * gate_sig
    hidden = (active * up_proj).astype(jnp.bfloat16)
    d_hidden = 0.5 * down_sum
    d_gate = (d_hidden * up_proj * gate_sig * (1.0 + gate * (1.0 - gate_sig))).astype(jnp.bfloat16)
    d_up = (d_hidden * active).astype(jnp.bfloat16)
    partial_value = lax.dot_general(
        d_gate, gate_full, contract_cols, preferred_element_type=jnp.float32
    ) + lax.dot_general(d_up, up_full, contract_cols, preferred_element_type=jnp.float32)
    summed_units = lax.psum(partial_value.astype(jnp.bfloat16), "tp")
    normalized_gradient = summed_units.astype(jnp.float32)
    gain_gradient = lax.psum(jnp.sum(normalized_gradient * unit_input, axis=0), ("rep", "fs"))
    gain_scaled = gain * normalized_gradient
    mean_correction = jnp.mean(gain_scaled * unit_input, axis=-1, keepdims=True)
    input_gradient = (
        cotangent.astype(jnp.float32)
        + reciprocal_root_mean * (gain_scaled - unit_input * mean_correction)
    ).astype(jnp.bfloat16)
    contract_rows = (((0,), (0,)), ((), ()))
    width = cotangent.shape[1]
    groups_fs = lax.axis_size("fs")
    groups_rep = lax.axis_size("rep")
    sub_rows = width // (groups_fs * groups_rep)
    reordered = (
        cotangent.reshape(row_count, groups_fs, groups_rep, sub_rows)
        .transpose(0, 2, 1, 3)
        .reshape(row_count, width)
    )
    summed = lax.psum_scatter(
        0.5 * lax.dot_general(reordered, hidden, contract_rows, preferred_element_type=jnp.float32),
        ("rep", "fs"),
        scatter_dimension=0,
        tiled=True,
    )
    d_down = lax.all_gather(summed, "rep", axis=0, tiled=True)
    return (input_gradient, gain_gradient, d_down)


def solution(mesh):
    placed = (
        P(("rep", "fs"), None),
        P(),
        P("fs", "tp"),
        P("fs", "tp"),
        P("fs", "tp"),
        P(("rep", "fs"), None),
    )
    return jax.shard_map(
        local,
        mesh=mesh,
        in_specs=placed,
        out_specs=(P(("rep", "fs"), None), P(), P("fs", "tp")),
        check_vma=False,
    )
```

profile of v0, /device:TPU:0, one launch (start us, length us, event | category | flops | bytes accessed | tf_op | source)
XLA Modules:
  0.0 600.7 jit_solution(4841965839708579481)
XLA Ops:
  7.2 0.7 all-gather.9.cloned.1.call-update
  8.0 0.7 all-gather.7.cloned.1.call-update
  8.7 0.7 all-gather.5.cloned.1.call-update
  9.5 2.5 copy.11
  12.0 3.3 copy.12
  15.2 0.5 fusion.9
  15.7 95.9 %all-gather.9.cloned.1.call-done = bf16[2048,1536]{1,0:T(8,128)(2,1)} async-done(((bf16[256,1536]{1,0:T(8,128)(2,1)}), bf16[2048,1536]{1,0:T(8,128)(2,1)}) %all-gather.9.cloned.1.call-update) | async-done | bytes 6291472 | tf_op jit(solution)/shard_map/all_gather | solution.py:19
  111.6 7.9 %fusion.14 = f32[512,1536]{1,0:T(8,128)} fusion(bf16[2048,1536]{1,0:T(8,128)(2,1)} %all-gather.9.cloned.1.call-done, bf16[512,2048]{1,0:T(8,128)(2,1)S(1)} %copy-done, f32[2048]{0:T(1024)S(1)} %copy-done.3, f32[512]{0:T(512)S(1)} %add_rsqrt_fusion), kind=kOutput, calls=%fused_computation.25 | convolution fusion | flops 3225419776 | bytes 11544576 | tf_op jit(solution)/shard_map/dot_general | solution.py:23
  119.5 91.2 %all-gather.7.cloned.1.call-done = bf16[2048,1536]{1,0:T(8,128)(2,1)} async-done(((bf16[256,1536]{1,0:T(8,128)(2,1)}), bf16[2048,1536]{1,0:T(8,128)(2,1)}) %all-gather.7.cloned.1.call-update) | async-done | bytes 6291472 | tf_op jit(solution)/shard_map/all_gather | solution.py:20
  210.7 5.8 fusion.16
  216.5 1.7 copy-done.6
  218.2 6.8 %multiply_bitcast_fusion = f32[2048,1536]{0,1:T(8,128)} fusion(bf16[512,2048]{0,1:T(8,128)(2,1)S(1)} %bitcast.14, f32[512,1536]{1,0:T(8,128)S(1)} %fusion.16, f32[512,1536]{1,0:T(8,128)S(1)} %copy-done.4), kind=kOutput, calls=%fused_computation | convolution fusion | flops 3229089792 | bytes 20971520 | tf_op jit(solution)/shard_map/dot_general | solution.py:55
  225.1 0.2 all-reduce.2.cloned.1.call-start
  225.3 84.5 %all-gather.5.cloned.1.call-done = bf16[2048,1536]{1,0:T(8,128)(2,1)} async-done(((bf16[256,1536]{1,0:T(8,128)(2,1)}), bf16[2048,1536]{1,0:T(8,128)(2,1)}) %all-gather.5.cloned.1.call-update) | async-done | bytes 6291472 | tf_op jit(solution)/shard_map/all_gather | solution.py:21
  309.8 8.6 %convolution_multiply_fusion = f32[512,1536]{1,0:T(8,128)} fusion(bf16[512,2048]{1,0:T(8,128)(2,1)} %param.11, bf16[2048,1536]{1,0:T(8,128)(2,1)} %all-gather.5.cloned.1.call-done), kind=kOutput, calls=%fused_computation.17 | convolution fusion | flops 3222011904 | bytes 11534336 | tf_op jit(solution)/shard_map/dot_general | solution.py:25
  318.4 8.6 %fusion.12 = f32[512,2048]{1,0:T(8,128)S(1)} fusion(bf16[2048,1536]{1,0:T(8,128)(2,1)} %all-gather.9.cloned.1.call-done, f32[512,1536]{1,0:T(8,128)S(1)} %copy-done.5, f32[512,1536]{1,0:T(8,128)} %convolution_multiply_fusion, f32[512,1536]{1,0:T(8,128)S(1)} %copy-done.7), kind=kOutput, calls=%fused_computation.23 | convolution fusion | flops 3229089792 | bytes 19922944 | tf_op jit(solution)/shard_map/dot_general | solution.py:32
  327.1 6.6 %add_convert_fusion = bf16[512,2048]{1,0:T(8,128)(2,1)} fusion(f32[512,2048]{1,0:T(8,128)S(1)} %fusion.12, bf16[2048,1536]{1,0:T(8,128)(2,1)S(1)} %bitcast.16, f32[512,1536]{1,0:T(8,128)} %convolution_multiply_fusion, f32[512,1536]{1,0:T(8,128)S(1)} %copy-done.5), kind=kOutput, calls=%fused_computation.16 | convolution fusion | flops 3228041216 | bytes 18874368 | tf_op jit(solution)/shard_map/dot_general | solution.py:34
  333.7 0.0 all-gather.11.cloned.1.call-start
  333.7 182.3 %reduce-scatter.2.cloned.1.call-done = f32[128,1536]{0,1:T(8,128)} async-done(((f32[2048,1536]{0,1:T(8,128)}), f32[128,1536]{0,1:T(8,128)}) %reduce-scatter.2.cloned.1.call-update) | async-done | bytes 786448 | tf_op jit(solution)/shard_map/reduce_scatter | solution.py:54
  516.1 23.6 %all-reduce.2.cloned.1.call-done = bf16[512,2048]{1,0:T(8,128)(2,1)} async-done(((bf16[512,2048]{1,0:T(8,128)(2,1)}), bf16[512,2048]{1,0:T(8,128)(2,1)}) %all-reduce.2.cloned.1.call-update) | async-done | bytes 2097168 | tf_op jit(solution)/shard_map/psum | solution.py:35
  539.6 2.9 fusion.10
  542.5 43.3 %psum.15 = f32[2048]{0:T(1024)} all-reduce(f32[2048]{0:T(1024)S(1)} %get-tuple-element.12), channel_id=1, replica_groups=mesh['rep'=2,'fs'=8,'tp'=2] {'rep','fs'}, use_global_device_ids=true, to_apply=%region_4.0 | all-reduce | flops 2048 | bytes 16384 | tf_op jit(solution)/shard_map/psum | solution.py:37
  585.8 5.0 fusion.6
  590.8 3.0 copy.13
  (30 shorter events, 0.3 us)
Async XLA Ops:
  7.2 2.3 copy-start.1
  7.2 104.4 %all-gather.9.cloned.1.call-start = ((), (), s32[]{:S(2)}) async-start(), calls=%async_computation.3 | async-start | bytes 7077888 | tf_op jit(solution)/shard_map/all_gather | solution.py:19
  7.9 202.8 %all-gather.7.cloned.1.call-start = ((), (), s32[]{:S(2)}) async-start(), calls=%async_computation.2 | async-start | bytes 7077888 | tf_op jit(solution)/shard_map/all_gather | solution.py:20
  8.7 301.1 %all-gather.5.cloned.1.call-start = ((), (), s32[]{:S(2)}) async-start(), calls=%async_computation.1 | async-start | bytes 7077888 | tf_op jit(solution)/shard_map/all_gather | solution.py:21
  9.4 506.6 %reduce-scatter.2.cloned.1.call-start = ((), (), s32[]{:S(2)}) async-start(), calls=%async_computation.5 | async-start | bytes 13369344 | tf_op jit(solution)/shard_map/reduce_scatter | solution.py:54
  12.0 3.3 copy-start
  12.0 99.7 %copy-start.3 = (f32[2048]{0:T(1024)S(1)}, f32[2048]{0:T(1024)}, u32[]{:S(2)}) copy-start(f32[2048]{0:T(1024)} %param.7) | copy-start | bytes 24580
  210.7 7.5 %copy-start.2 = (bf16[512,2,8,128]{0,3,2,1:T(8,128)(2,1)S(1)}, bf16[512,2,8,128]{0,3,2,1:T(8,128)(2,1)}, u32[]{:S(2)}) copy-start(bf16[512,2,8,128]{0,3,2,1:T(8,128)(2,1)} %copy.12) | copy-start | bytes 6291460
  210.7 7.5 %copy-start.4 = (f32[512,1536]{1,0:T(8,128)S(1)}, f32[512,1536]{1,0:T(8,128)}, u32[]{:S(2)}) copy-start(f32[512,1536]{1,0:T(8,128)} %fusion.14) | copy-start | bytes 9437188
  216.5 1.8 copy-start.6
  225.1 314.5 %all-reduce.2.cloned.1.call-start = ((), (), s32[]{:S(2)}) async-start(), calls=%async_computation.4 | async-start | bytes 4194304 | tf_op jit(solution)/shard_map/psum | solution.py:35
  309.8 8.6 %copy-start.5 = (f32[512,1536]{1,0:T(8,128)S(1)}, f32[512,1536]{1,0:T(8,128)}, u32[]{:S(2)}) copy-start(f32[512,1536]{1,0:T(8,128)} %fusion.14) | copy-start | bytes 9437188
  309.8 8.6 %copy-start.7 = (f32[512,1536]{1,0:T(8,128)S(1)}, f32[512,1536]{1,0:T(8,128)}, u32[]{:S(2)}) copy-start(f32[512,1536]{1,0:T(8,128)} %copy-done.6) | copy-start | bytes 9437188
  309.8 17.2 %slice-start = ((s8[6291456]{0:T(1024)(128)(4,1)}), s8[4194304]{0:T(1024)(128)(4,1)S(1)}, s32[]{:S(2)}) async-start(s8[6291456]{0:T(1024)(128)(4,1)} %bitcast.15), calls=%async_computation.7 | async-start | bytes 8388608
  318.4 8.6 %slice-start.1 = ((s8[6291456]{0:T(1024)(128)(4,1)}), s8[2097152]{0:T(1024)(128)(4,1)S(1)}, s32[]{:S(2)}) async-start(s8[6291456]{0:T(1024)(128)(4,1)} %bitcast.15), calls=%async_computation.8 | async-start | bytes 4194304
  333.7 257.1 %all-gather.11.cloned.1.call-start = ((), (), s32[]{:S(2)}) async-start(), calls=%async_computation.6 | async-start | bytes 2359296 | tf_op jit(solution)/shard_map/all_gather | solution.py:60
Sparse Core Ops, SparseCore 0:
  10.2 101.4 all-gather.8
  113.8 96.8 all-gather.6
  212.9 96.8 all-gather.4
  315.3 200.6 reduce-scatter.1
  518.8 20.7 all-reduce.1
  541.0 28.3 all-gather.10
where the time goes:
time: 601 us
  waiting for transfers between devices  480 us (80%)
  matrix products  44.2 us (7%)
  blocking collectives  43.3 us (7%)
  between operations  14.2 us (2%)
  local copies, waits for them, and re-layouts  10.6 us (2%)
  other arithmetic  8.39 us (1%)
    reduce_scatter x1, waiting for transfers between devices, local(): lax.psum_scatter(0.5 * lax.dot_general(reordered, hidden, contract_rows,...  182 us
    all_gather x1, waiting for transfers between devices, local(): lax.all_gather(gate_weight, 'fs', axis=0, tiled=True)  95.9 us
    all_gather x1, waiting for transfers between devices, local(): lax.all_gather(up_weight, 'fs', axis=0, tiled=True)  91.2 us
    all_gather x1, waiting for transfers between devices, local(): lax.all_gather(down_weight, 'fs', axis=0, tiled=True)  84.5 us
    psum x1, blocking collectives, local(): lax.psum(jnp.sum(normalized_gradient * unit_input, axis=0), ('rep', 'fs'))  43.3 us
    psum x1, waiting for transfers between devices, local(): summed_units = lax.psum(partial_value.astype(jnp.bfloat16), 'tp')  23.6 us
  transfers between devices with their start and end apart: 6, of which 5 were waited for; matrix products, arithmetic and copies ran while one was open for 10% of the time, Pallas kernels for 0%

commit v1 on v0

--- a/solution.py
+++ b/solution.py
@@ -34,7 +34,9 @@
     ) + lax.dot_general(d_up, up_full, contract_cols, preferred_element_type=jnp.float32)
     summed_units = lax.psum(partial_value.astype(jnp.bfloat16), "tp")
     normalized_gradient = summed_units.astype(jnp.float32)
-    gain_gradient = lax.psum(jnp.sum(normalized_gradient * unit_input, axis=0), ("rep", "fs"))
+    gain_gradient = lax.psum(
+        lax.psum(jnp.sum(normalized_gradient * unit_input, axis=0), axis_name="fs"), axis_name="rep"
+    )
     gain_scaled = gain * normalized_gradient
     mean_correction = jnp.mean(gain_scaled * unit_input, axis=-1, keepdims=True)
     input_gradient = (

time: 601 us -> 585 us (0.973)
  blocking collectives: 43.3 us -> 27.5 us
    psum x1 -> x2, blocking collectives: 43.3 us -> 27.5 us  [the longest x1 21.9 us: local(): lax.psum(jnp.sum(normalized_gradient * unit_input, axis=0), axis_name='fs')]
where the time goes in v1:
time: 585 us
  waiting for transfers between devices  480 us (82%)
  matrix products  44.3 us (8%)
  blocking collectives  27.5 us (5%)
  between operations  14.2 us (2%)
  local copies, waits for them, and re-layouts  10.6 us (2%)
  other arithmetic  8.4 us (1%)
    reduce_scatter x1, waiting for transfers between devices, local(): lax.psum_scatter(0.5 * lax.dot_general(reordered, hidden, contract_rows,...  182 us
    all_gather x1, waiting for transfers between devices, local(): lax.all_gather(gate_weight, 'fs', axis=0, tiled=True)  95.9 us
    all_gather x1, waiting for transfers between devices, local(): lax.all_gather(up_weight, 'fs', axis=0, tiled=True)  91.2 us
    all_gather x1, waiting for transfers between devices, local(): lax.all_gather(down_weight, 'fs', axis=0, tiled=True)  84.4 us
    psum x1, waiting for transfers between devices, local(): summed_units = lax.psum(partial_value.astype(jnp.bfloat16), 'tp')  23.5 us
    psum x1, blocking collectives, local(): lax.psum(jnp.sum(normalized_gradient * unit_input, axis=0), axis_name='fs')  21.9 us
  transfers between devices with their start and end apart: 6, of which 5 were waited for; matrix products, arithmetic and copies ran while one was open for 10% of the time, Pallas kernels for 0%

profile of v1, /device:TPU:0, one launch (start us, length us, event | category | flops | bytes accessed | tf_op | source)
XLA Modules:
  0.0 584.9 jit_solution(11957123939218448352)
XLA Ops:
  7.2 0.7 all-gather.9.cloned.1.call-update
  8.0 0.7 all-gather.7.cloned.1.call-update
  8.7 0.7 all-gather.5.cloned.1.call-update
  9.5 2.5 copy.11
  12.0 3.3 copy.12
  15.2 0.5 fusion.9
  15.7 95.9 %all-gather.9.cloned.1.call-done = bf16[2048,1536]{1,0:T(8,128)(2,1)} async-done(((bf16[256,1536]{1,0:T(8,128)(2,1)}), bf16[2048,1536]{1,0:T(8,128)(2,1)}) %all-gather.9.cloned.1.call-update) | async-done | bytes 6291472 | tf_op jit(solution)/shard_map/all_gather | solution.py:19
  111.6 7.9 %fusion.14 = f32[512,1536]{1,0:T(8,128)} fusion(bf16[2048,1536]{1,0:T(8,128)(2,1)} %all-gather.9.cloned.1.call-done, bf16[512,2048]{1,0:T(8,128)(2,1)S(1)} %copy-done, f32[2048]{0:T(1024)S(1)} %copy-done.3, f32[512]{0:T(512)S(1)} %add_rsqrt_fusion), kind=kOutput, calls=%fused_computation.25 | convolution fusion | flops 3225419776 | bytes 11544576 | tf_op jit(solution)/shard_map/dot_general | solution.py:23
  119.5 91.2 %all-gather.7.cloned.1.call-done = bf16[2048,1536]{1,0:T(8,128)(2,1)} async-done(((bf16[256,1536]{1,0:T(8,128)(2,1)}), bf16[2048,1536]{1,0:T(8,128)(2,1)}) %all-gather.7.cloned.1.call-update) | async-done | bytes 6291472 | tf_op jit(solution)/shard_map/all_gather | solution.py:20
  210.7 5.8 fusion.16
  216.5 1.7 copy-done.6
  218.2 6.9 %multiply_bitcast_fusion = f32[2048,1536]{0,1:T(8,128)} fusion(bf16[512,2048]{0,1:T(8,128)(2,1)S(1)} %bitcast.14, f32[512,1536]{1,0:T(8,128)S(1)} %fusion.16, f32[512,1536]{1,0:T(8,128)S(1)} %copy-done.4), kind=kOutput, calls=%fused_computation | convolution fusion | flops 3229089792 | bytes 20971520 | tf_op jit(solution)/shard_map/dot_general | solution.py:57
  225.2 0.2 all-reduce.2.cloned.1.call-start
  225.4 84.4 %all-gather.5.cloned.1.call-done = bf16[2048,1536]{1,0:T(8,128)(2,1)} async-done(((bf16[256,1536]{1,0:T(8,128)(2,1)}), bf16[2048,1536]{1,0:T(8,128)(2,1)}) %all-gather.5.cloned.1.call-update) | async-done | bytes 6291472 | tf_op jit(solution)/shard_map/all_gather | solution.py:21
  309.8 8.6 %convolution_multiply_fusion = f32[512,1536]{1,0:T(8,128)} fusion(bf16[512,2048]{1,0:T(8,128)(2,1)} %param.11, bf16[2048,1536]{1,0:T(8,128)(2,1)} %all-gather.5.cloned.1.call-done), kind=kOutput, calls=%fused_computation.17 | convolution fusion | flops 3222011904 | bytes 11534336 | tf_op jit(solution)/shard_map/dot_general | solution.py:25
  318.4 8.6 %fusion.12 = f32[512,2048]{1,0:T(8,128)S(1)} fusion(bf16[2048,1536]{1,0:T(8,128)(2,1)} %all-gather.9.cloned.1.call-done, f32[512,1536]{1,0:T(8,128)S(1)} %copy-done.5, f32[512,1536]{1,0:T(8,128)} %convolution_multiply_fusion, f32[512,1536]{1,0:T(8,128)S(1)} %copy-done.7), kind=kOutput, calls=%fused_computation.23 | convolution fusion | flops 3229089792 | bytes 19922944 | tf_op jit(solution)/shard_map/dot_general | solution.py:32
  327.0 6.6 %add_convert_fusion = bf16[512,2048]{1,0:T(8,128)(2,1)} fusion(f32[512,2048]{1,0:T(8,128)S(1)} %fusion.12, bf16[2048,1536]{1,0:T(8,128)(2,1)S(1)} %bitcast.16, f32[512,1536]{1,0:T(8,128)} %convolution_multiply_fusion, f32[512,1536]{1,0:T(8,128)S(1)} %copy-done.5), kind=kOutput, calls=%fused_computation.16 | convolution fusion | flops 3228041216 | bytes 18874368 | tf_op jit(solution)/shard_map/dot_general | solution.py:34
  333.7 182.4 %reduce-scatter.2.cloned.1.call-done = f32[128,1536]{0,1:T(8,128)} async-done(((f32[2048,1536]{0,1:T(8,128)}), f32[128,1536]{0,1:T(8,128)}) %reduce-scatter.2.cloned.1.call-update) | async-done | bytes 786448 | tf_op jit(solution)/shard_map/reduce_scatter | solution.py:56
  516.1 23.5 %all-reduce.2.cloned.1.call-done = bf16[512,2048]{1,0:T(8,128)(2,1)} async-done(((bf16[512,2048]{1,0:T(8,128)(2,1)}), bf16[512,2048]{1,0:T(8,128)(2,1)}) %all-reduce.2.cloned.1.call-update) | async-done | bytes 2097168 | tf_op jit(solution)/shard_map/psum | solution.py:35
  539.7 2.9 fusion.10
  542.6 21.9 %psum.22 = f32[2048]{0:T(1024)S(1)} all-reduce(f32[2048]{0:T(1024)S(1)} %get-tuple-element.12), channel_id=1, replica_groups=mesh['rep'=2,'fs'=8,'tp'=2] {'fs'}, use_global_device_ids=true, to_apply=%region_4.0 | all-reduce | flops 2048 | bytes 16384 | tf_op jit(solution)/shard_map/psum | solution.py:38
  564.5 5.6 psum.23
  570.1 5.0 fusion.6
  575.1 3.0 copy.13
  (31 shorter events, 0.3 us)
Async XLA Ops:
  7.2 2.3 copy-start.1
  7.2 104.4 %all-gather.9.cloned.1.call-start = ((), (), s32[]{:S(2)}) async-start(), calls=%async_computation.3 | async-start | bytes 7077888 | tf_op jit(solution)/shard_map/all_gather | solution.py:19
  7.9 202.8 %all-gather.7.cloned.1.call-start = ((), (), s32[]{:S(2)}) async-start(), calls=%async_computation.2 | async-start | bytes 7077888 | tf_op jit(solution)/shard_map/all_gather | solution.py:20
  8.7 301.1 %all-gather.5.cloned.1.call-start = ((), (), s32[]{:S(2)}) async-start(), calls=%async_computation.1 | async-start | bytes 7077888 | tf_op jit(solution)/shard_map/all_gather | solution.py:21
  9.4 506.7 %reduce-scatter.2.cloned.1.call-start = ((), (), s32[]{:S(2)}) async-start(), calls=%async_computation.5 | async-start | bytes 13369344 | tf_op jit(solution)/shard_map/reduce_scatter | solution.py:56
  12.0 3.3 copy-start
  12.0 99.7 %copy-start.3 = (f32[2048]{0:T(1024)S(1)}, f32[2048]{0:T(1024)}, u32[]{:S(2)}) copy-start(f32[2048]{0:T(1024)} %param.7) | copy-start | bytes 24580
  210.7 7.5 %copy-start.2 = (bf16[512,2,8,128]{0,3,2,1:T(8,128)(2,1)S(1)}, bf16[512,2,8,128]{0,3,2,1:T(8,128)(2,1)}, u32[]{:S(2)}) copy-start(bf16[512,2,8,128]{0,3,2,1:T(8,128)(2,1)} %copy.12) | copy-start | bytes 6291460
  210.7 7.5 %copy-start.4 = (f32[512,1536]{1,0:T(8,128)S(1)}, f32[512,1536]{1,0:T(8,128)}, u32[]{:S(2)}) copy-start(f32[512,1536]{1,0:T(8,128)} %fusion.14) | copy-start | bytes 9437188
  216.5 1.8 copy-start.6
  225.2 314.5 %all-reduce.2.cloned.1.call-start = ((), (), s32[]{:S(2)}) async-start(), calls=%async_computation.4 | async-start | bytes 4194304 | tf_op jit(solution)/shard_map/psum | solution.py:35
  309.8 8.6 %copy-start.5 = (f32[512,1536]{1,0:T(8,128)S(1)}, f32[512,1536]{1,0:T(8,128)}, u32[]{:S(2)}) copy-start(f32[512,1536]{1,0:T(8,128)} %fusion.14) | copy-start | bytes 9437188
  309.8 8.6 %copy-start.7 = (f32[512,1536]{1,0:T(8,128)S(1)}, f32[512,1536]{1,0:T(8,128)}, u32[]{:S(2)}) copy-start(f32[512,1536]{1,0:T(8,128)} %copy-done.6) | copy-start | bytes 9437188
  309.8 17.2 %slice-start = ((s8[6291456]{0:T(1024)(128)(4,1)}), s8[4194304]{0:T(1024)(128)(4,1)S(1)}, s32[]{:S(2)}) async-start(s8[6291456]{0:T(1024)(128)(4,1)} %bitcast.15), calls=%async_computation.7 | async-start | bytes 8388608
  318.4 8.6 %slice-start.1 = ((s8[6291456]{0:T(1024)(128)(4,1)}), s8[2097152]{0:T(1024)(128)(4,1)S(1)}, s32[]{:S(2)}) async-start(s8[6291456]{0:T(1024)(128)(4,1)} %bitcast.15), calls=%async_computation.8 | async-start | bytes 4194304
  333.6 241.4 %all-gather.11.cloned.1.call-start = ((), (), s32[]{:S(2)}) async-start(), calls=%async_computation.6 | async-start | bytes 2359296 | tf_op jit(solution)/shard_map/all_gather | solution.py:62
Sparse Core Ops, SparseCore 0:
  10.2 101.4 all-gather.8
  113.8 96.8 all-gather.6
  212.9 96.8 all-gather.4
  315.3 200.7 reduce-scatter.1
  518.9 20.7 all-reduce.1
  541.1 28.4 all-gather.10
